TPU v7x, 32 devices: a whole 2x2x4 slice. The times are simulated.
32 devices in a mesh: sp: 8 (over z, x), tp: 4 (over y, core).
Axes of the slice: x: 2, y: 2, z: 4, core: 2. Of those that a mesh axis runs over, the one named last changes fastest.
Arguments:
- residual: bfloat16 [4096, 2048], P('sp'), may hold values from -80 to 80
- queries: bfloat16 [4096, 1024], P('sp', 'tp'), may hold values from -260 to 260
- keys: bfloat16 [4096, 512], P('sp', 'tp'), may hold values from -7 to 7
- values: bfloat16 [4096, 512], P('sp', 'tp'), may hold values from -12 to 12
- documents: int32 [4096], P('sp'), may hold values from 0 to 3, never falling along the last dimension, each value on 1 to 3072 neighbouring positions
- sinks: float32 [16], P('tp'), may hold values from 1 to 6
- out_weight: bfloat16 [1024, 2048], P('tp'), may hold values from -0.5 to 0.5
- norm_gain: float32 [2048], replicated, may hold values from 0.1 to 1.9
- gate_weight: bfloat16 [2048, 5632], P('sp', 'tp'), may hold values from -0.125 to 0.125
- up_weight: bfloat16 [2048, 5632], P('sp', 'tp'), may hold values from -0.125 to 0.125
- down_weight: bfloat16 [2048, 5632], P('sp', 'tp'), may hold values from -0.078125 to 0.078125
Outputs:
- mixed: bfloat16 [4096, 2048], P('sp', 'tp')
Inputs may be any that keep to these rules, and one draw needn't show every extreme that they name: `documents`: document numbers never fall along the positions; a document holds at most 3072 positions.
All inputs are finite; a program needn't handle non-finite values.
Results may differ from a plain program's by a relative error of at most 0.01.
Values may be sent and summed in bfloat16 or wider, within the bound.
A program may use at most 64 MiB of HBM per device.

v0:
```python
import jax
import jax.numpy as jnp
from jax import lax
from jax.sharding import PartitionSpec as P

HEAD_DIM = 64
WINDOW = 128
GROUP = 2
neg_big = -1e30
norm_eps = 1e-05


def from_behind(shard, axis, by):
    length = lax.axis_size(axis)
    pairs = [(i, i + by) for i in range(length) if 0 <= i + by < length]
    return lax.ppermute(shard, axis, pairs)


def attend(queries, keys, values, documents, sinks, tail_keys, tail_values, tail_docs, offset):
    rows_here = queries.shape[0]
    block_count = rows_here // WINDOW
    kv_here = keys.shape[1] // HEAD_DIM
    q_blocks = queries.reshape(block_count, WINDOW, kv_here, GROUP, HEAD_DIM)
    k_blocks = keys.reshape(block_count, WINDOW, kv_here, HEAD_DIM)
    v_blocks = values.reshape(block_count, WINDOW, kv_here, HEAD_DIM)
    k_prev = jnp.concatenate(
        [tail_keys.reshape(1, WINDOW, kv_here, HEAD_DIM), k_blocks[:-1]], axis=0
    )
    v_prev = jnp.concatenate(
        [tail_values.reshape(1, WINDOW, kv_here, HEAD_DIM), v_blocks[:-1]], axis=0
    )
    k_band = jnp.concatenate([k_prev, k_blocks], axis=1)
    v_band = jnp.concatenate([v_prev, v_blocks], axis=1)
    doc_own = documents.astype(jnp.float32).reshape(block_count, WINDOW)
    doc_prev = jnp.concatenate(
        [tail_docs.astype(jnp.float32).reshape(1, WINDOW), doc_own[:-1]], axis=0
    )
    doc_band = jnp.concatenate([doc_prev, doc_own], axis=1)
    row_idx = jnp.arange(WINDOW, dtype=jnp.int32)
    col_idx = jnp.arange(2 * WINDOW, dtype=jnp.int32)
    first = offset + jnp.arange(block_count, dtype=jnp.int32) * WINDOW
    q_pos = first[:, None] + row_idx[None, :]
    k_pos = first[:, None] - WINDOW + col_idx[None, :]
    distance = q_pos[:, :, None] - k_pos[:, None, :]
    visible = (
        (distance >= 0)
        & (distance < WINDOW)
        & (k_pos[:, None, :] >= 0)
        & (doc_own[:, :, None] == doc_band[:, None, :])
    )
    scores = jnp.einsum(
        "nikgd,njkd->nkgij", q_blocks, k_band, preferred_element_type=jnp.float32
    ) * HEAD_DIM ** (-0.5)
    scores = jnp.where(visible[:, None, None], scores, neg_big)
    sink_logit = sinks.reshape(1, kv_here, GROUP, 1, 1)
    row_max = jnp.maximum(scores.max(-1, keepdims=True), sink_logit)
    expo = jnp.where(visible[:, None, None], jnp.exp(scores - row_max), 0.0)
    denom_sum = expo.sum(-1, keepdims=True) + jnp.exp(sink_logit - row_max)
    weights = (expo / denom_sum).astype(jnp.bfloat16)
    mixed = jnp.einsum("nkgij,njkd->nikgd", weights, v_band, preferred_element_type=jnp.float32)
    return mixed.reshape(rows_here, kv_here * GROUP * HEAD_DIM).astype(jnp.bfloat16)


def on_device(
    residual,
    queries,
    keys,
    values,
    documents,
    sinks,
    out_weight,
    norm_gain,
    gate_weight,
    up_weight,
    down_weight,
):
    rows_here = queries.shape[0]
    offset = lax.axis_index("sp") * rows_here
    doc_tail = documents[rows_here - WINDOW :].astype(jnp.bfloat16)
    tail_keys, tail_values, tail_docs = from_behind(
        (keys[rows_here - WINDOW :], values[rows_here - WINDOW :], doc_tail), "sp", 1
    )
    attended = attend(
        queries, keys, values, documents, sinks, tail_keys, tail_values, tail_docs, offset
    )
    model_width = residual.shape[1]
    col_count = model_width // lax.axis_size("tp")
    col_first = lax.axis_index("tp") * col_count
    full_term = jnp.dot(attended, out_weight, preferred_element_type=jnp.float32)
    projected = lax.psum(full_term.astype(jnp.bfloat16), "tp").astype(jnp.float32)
    after_full = (residual.astype(jnp.float32) + projected).astype(jnp.bfloat16)
    after_f = after_full.astype(jnp.float32)
    inv_rms = lax.rsqrt(jnp.mean(after_f * after_f, axis=1, keepdims=True) + norm_eps)
    normed = (after_f * inv_rms * norm_gain[None, :]).astype(jnp.bfloat16)
    after = lax.dynamic_slice_in_dim(after_full, col_first, col_count, 1)
    gate_act = jnp.dot(
        normed,
        lax.all_gather(gate_weight, "sp", axis=0, tiled=True),
        preferred_element_type=jnp.float32,
    )
    up_act = jnp.dot(
        normed,
        lax.all_gather(up_weight, "sp", axis=0, tiled=True),
        preferred_element_type=jnp.float32,
    )
    down_full = lax.all_gather(down_weight, "sp", axis=0, tiled=True)
    hidden = (jax.nn.silu(gate_act) * up_act).astype(jnp.bfloat16)
    summed = lax.psum_scatter(
        lax.dot_general(
            down_full, hidden, (((1,), (1,)), ((), ())), preferred_element_type=jnp.float32
        ).astype(jnp.bfloat16),
        "tp",
        scatter_dimension=0,
        tiled=True,
    ).astype(jnp.float32)
    return (after.astype(jnp.float32) + summed.T).astype(jnp.bfloat16)


def solution(mesh):
    return jax.shard_map(
        on_device,
        mesh=mesh,
        in_specs=(
            P("sp", None),
            P("sp", "tp"),
            P("sp", "tp"),
            P("sp", "tp"),
            P("sp"),
            P("tp"),
            P("tp", None),
            P(),
            P("sp", "tp"),
            P("sp", "tp"),
            P("sp", "tp"),
        ),
        out_specs=P("sp", "tp"),
        check_vma=False,
    )
```

profile of v0, /device:TPU:0, one launch (start us, length us, event | category | flops | bytes accessed | tf_op | source)
XLA Modules:
  0.0 367.5 jit_solution(8054649888373592953)
XLA Ops:
  7.4 0.8 fusion.34
  8.2 4.9 %collective-permute-start.1 = (bf16[128]{0:T(256)(128)(2,1)S(1)}, bf16[128]{0:T(256)(128)(2,1)S(1)}, u32[]{:S(2)}, u32[]{:S(2)}) collective-permute-start(bf16[128]{0:T(256)(128)(2,1)S(1)} %slice.39), channel_id=1, source_target_pairs={{0,4},{4,8},{8,12},{12,16},{16,20},{20,24},{24,28},{1,5},{5,9},{9,... | collective-permute-start | bytes 776 | tf_op jit(solution)/shard_map/ppermute | solution.py:16
  13.1 0.8 slice.42
  13.9 3.4 collective-permute-start.2
  17.3 1.4 slice.36
  18.7 4.0 %collective-permute-start = (bf16[128,128]{1,0:T(8,128)(2,1)}, bf16[128,128]{1,0:T(8,128)(2,1)}, u32[]{:S(2)}, u32[]{:S(2)}) collective-permute-start(bf16[128,128]{1,0:T(8,128)(2,1)} %slice.36), channel_id=1, source_target_pairs={{0,4},{4,8},{8,12},{12,16},{16,20},{20,24},{24,28},{1,5},{5,9},{9,... | collective-permute-start | bytes 98312 | tf_op jit(solution)/shard_map/ppermute | solution.py:16
  22.8 1.0 reshape.148
  23.9 1.0 reshape.146
  25.0 2.0 reshape.149
  27.1 0.8 copy.23
  28.3 0.8 copy.18
  29.2 0.6 fusion.17
  29.8 0.7 copy.21
  30.5 1.6 fusion.5
  32.3 0.5 fusion.6
  32.9 0.9 copy.16
  33.8 0.7 fusion.7
  34.5 0.2 copy.29
  34.7 2.1 convolution_convert_fusion
  36.9 0.5 all-gather.4.cloned.1.call-update
  37.4 0.5 all-gather.6.cloned.1.call-update
  38.0 0.5 all-gather.8.cloned.1.call-update
  38.6 0.2 reduce-scatter.2.cloned.1.call-start
  38.8 48.3 %all-reduce.2.cloned.1.call-done = bf16[512,2048]{1,0:T(8,128)(2,1)} async-done(((bf16[512,2048]{1,0:T(8,128)(2,1)}), bf16[512,2048]{1,0:T(8,128)(2,1)}) %all-reduce.2.cloned.1.call-update) | async-done | bytes 2097168 | tf_op jit(solution)/shard_map/psum | solution.py:90
  87.1 3.2 fusion
  90.3 40.1 %all-gather.4.cloned.1.call-done = bf16[2048,1408]{1,0:T(8,128)(2,1)} async-done(((bf16[256,1408]{1,0:T(8,128)(2,1)}), bf16[2048,1408]{1,0:T(8,128)(2,1)}) %all-gather.4.cloned.1.call-update) | async-done | bytes 5767184 | tf_op jit(solution)/shard_map/all_gather | solution.py:98
  130.4 7.6 %fusion.11 = f32[512,1408]{1,0:T(8,128)} fusion(bf16[2048,1408]{1,0:T(8,128)(2,1)} %all-gather.4.cloned.1.call-done, bf16[512,2048]{1,0:T(8,128)(2,1)S(1)} %get-tuple-element.6, f32[2048]{0:T(1024)S(1)} %copy-done.2, f32[512]{0:T(512)S(1)} %add_rsqrt_fusion), kind=kOutput, calls=%fused_computation.22 | convolution fusion | flops 2956984320 | bytes 10758144 | tf_op jit(solution)/shard_map/dot_general | solution.py:96
  138.0 84.7 %all-gather.6.cloned.1.call-done = bf16[2048,1408]{1,0:T(8,128)(2,1)} async-done(((bf16[256,1408]{1,0:T(8,128)(2,1)}), bf16[2048,1408]{1,0:T(8,128)(2,1)}) %all-gather.6.cloned.1.call-update) | async-done | bytes 5767184 | tf_op jit(solution)/shard_map/all_gather | solution.py:103
  222.7 92.4 %all-gather.8.cloned.1.call-done = bf16[2048,1408]{1,0:T(8,128)(2,1)} async-done(((bf16[256,1408]{1,0:T(8,128)(2,1)}), bf16[2048,1408]{1,0:T(8,128)(2,1)}) %all-gather.8.cloned.1.call-update) | async-done | bytes 5767184 | tf_op jit(solution)/shard_map/all_gather | solution.py:106
  315.1 13.4 %fusion.4 = bf16[2048,512]{0,1:T(8,128)(2,1)} fusion(bf16[2048,1408]{1,0:T(8,128)(2,1)} %all-gather.8.cloned.1.call-done, bf16[2048,1408]{1,0:T(8,128)(2,1)} %all-gather.6.cloned.1.call-done, f32[512,1408]{1,0:T(8,128)} %fusion.11, bf16[512,2048]{1,0:T(8,128)(2,1)S(1)} %get-tuple-element.6, f32[2048]{0:T(1024)S(1)} %copy-done.2, f32[512]{0:T(512)S(1)} %add_rsqrt_fusion), kind=kOutput, calls=%fused_computation.10 | convolution fusion | flops 5915148288 | bytes 18622464 | tf_op jit(solution)/shard_map/dot_general | solution.py:109
  328.5 29.5 %reduce-scatter.2.cloned.1.call-done = bf16[512,512]{0,1:T(8,128)(2,1)} async-done(((bf16[2048,512]{0,1:T(8,128)(2,1)}), bf16[512,512]{0,1:T(8,128)(2,1)}) %reduce-scatter.2.cloned.1.call-update) | async-done | bytes 524304 | tf_op jit(solution)/shard_map/reduce_scatter | solution.py:108
  358.0 2.0 fusion.8
  (37 shorter events, 1.2 us)
Async XLA Ops:
  7.4 27.3 %copy-start = (bf16[256,2048]{1,0:T(8,128)(2,1)S(1)}, bf16[256,2048]{1,0:T(8,128)(2,1)}, u32[]{:S(2)}) copy-start(bf16[256,2048]{1,0:T(8,128)(2,1)} %param.17) | copy-start | bytes 3145732
  7.4 19.6 %slice-start = ((bf16[512,128]{1,0:T(8,128)(2,1)}), bf16[384,128]{1,0:T(8,128)(2,1)S(1)}, s32[]{:S(2)}) async-start(bf16[512,128]{1,0:T(8,128)(2,1)} %param.13), calls=%async_computation.6 | async-start | bytes 196608 | tf_op jit(solution)/shard_map/slice | solution.py:27
  7.4 20.8 %slice-start.1 = ((bf16[512,128]{1,0:T(8,128)(2,1)}), bf16[384,128]{1,0:T(8,128)(2,1)S(1)}, s32[]{:S(2)}) async-start(bf16[512,128]{1,0:T(8,128)(2,1)} %param.14), calls=%async_computation.7 | async-start | bytes 196608 | tf_op jit(solution)/shard_map/slice | solution.py:30
  7.4 20.7 %copy-start.3 = (f32[4]{0:T(128)S(1)}, f32[4]{0:T(128)}, u32[]{:S(2)}) copy-start(f32[4]{0:T(128)} %param.16) | copy-start | bytes 52
  7.4 79.7 %all-reduce.2.cloned.1.call-start = ((), (), s32[]{:S(2)}) async-start(), calls=%async_computation.1 | async-start | bytes 4194304 | tf_op jit(solution)/shard_map/psum | solution.py:90
  8.2 21.0 %collective-permute-start.1 = (bf16[128]{0:T(256)(128)(2,1)S(1)}, bf16[128]{0:T(256)(128)(2,1)S(1)}, u32[]{:S(2)}, u32[]{:S(2)}) collective-permute-start(bf16[128]{0:T(256)(128)(2,1)S(1)} %slice.39), channel_id=1, source_target_pairs={{0,4},{4,8},{8,12},{12,16},{16,20},{20,24},{24,28},{1,5},{5,9},{9,... | collective-permute-start | bytes 776 | tf_op jit(solution)/shard_map/ppermute | solution.py:16
  13.9 16.0 %collective-permute-start.2 = (bf16[128,128]{1,0:T(8,128)(2,1)S(1)}, bf16[128,128]{1,0:T(8,128)(2,1)S(1)}, u32[]{:S(2)}, u32[]{:S(2)}) collective-permute-start(bf16[128,128]{1,0:T(8,128)(2,1)S(1)} %slice.42), channel_id=1, source_target_pairs={{0,4},{4,8},{8,12},{12,16},{16,20},{20,24},{24,28},{1,5},{5,9},{9,... | collective-permute-start | bytes 98312 | tf_op jit(solution)/shard_map/ppermute | solution.py:16
  18.7 14.2 %collective-permute-start = (bf16[128,128]{1,0:T(8,128)(2,1)}, bf16[128,128]{1,0:T(8,128)(2,1)}, u32[]{:S(2)}, u32[]{:S(2)}) collective-permute-start(bf16[128,128]{1,0:T(8,128)(2,1)} %slice.36), channel_id=1, source_target_pairs={{0,4},{4,8},{8,12},{12,16},{16,20},{20,24},{24,28},{1,5},{5,9},{9,... | collective-permute-start | bytes 98312 | tf_op jit(solution)/shard_map/ppermute | solution.py:16
  32.2 1.6 copy-start.1
  36.8 93.5 %all-gather.4.cloned.1.call-start = ((), (), s32[]{:S(2)}) async-start(), calls=%async_computation.2 | async-start | bytes 6488064 | tf_op jit(solution)/shard_map/all_gather | solution.py:98
  37.4 185.3 %all-gather.6.cloned.1.call-start = ((), (), s32[]{:S(2)}) async-start(), calls=%async_computation.3 | async-start | bytes 6488064 | tf_op jit(solution)/shard_map/all_gather | solution.py:103
  38.0 277.1 %all-gather.8.cloned.1.call-start = ((), (), s32[]{:S(2)}) async-start(), calls=%async_computation.4 | async-start | bytes 6488064 | tf_op jit(solution)/shard_map/all_gather | solution.py:106
  38.6 91.8 %copy-start.2 = (f32[2048]{0:T(1024)S(1)}, f32[2048]{0:T(1024)}, u32[]{:S(2)}) copy-start(f32[2048]{0:T(1024)} %param.18) | copy-start | bytes 24580
  38.6 319.4 %reduce-scatter.2.cloned.1.call-start = ((), (), s32[]{:S(2)}) async-start(), calls=%async_computation.5 | async-start | bytes 2621440 | tf_op jit(solution)/shard_map/reduce_scatter | solution.py:108
Sparse Core Ops, SparseCore 0:
  36.9 50.1 all-reduce.1
  328.6 29.2 reduce-scatter.1
Sparse Core Ops, SparseCore 1:
  39.5 90.8 all-gather.3
  132.4 90.2 all-gather.5
  224.8 90.2 all-gather.7
where the time goes:
time: 368 us
  waiting for transfers between devices  296 us (80%)
  matrix products  25.5 us (7%)
  between operations  15.2 us (4%)
  starting transfers between devices  12.7 us (3%)
  local copies, waits for them, and re-layouts  10.2 us (3%)
  other arithmetic  7.52 us (2%)
    all_gather x1, waiting for transfers between devices, on_device(): down_full = lax.all_gather(down_weight, 'sp', axis=0, tiled=True)  92.4 us
    all_gather x1, waiting for transfers between devices, on_device(): lax.all_gather(up_weight, 'sp', axis=0, tiled=True)  84.7 us
    psum x1, waiting for transfers between devices, on_device(): lax.psum(full_term.astype(jnp.bfloat16), 'tp').astype(jnp.float32)  48.3 us
    all_gather x1, waiting for transfers between devices, on_device(): lax.all_gather(gate_weight, 'sp', axis=0, tiled=True)  40.1 us
    reduce_scatter x1, waiting for transfers between devices, on_device(): lax.psum_scatter(lax.dot_general(down_full, hidden, (((1,), (1,)), ((), (...  29.5 us
    dot_general x1, matrix products, on_device(): lax.dot_general(down_full, hidden, (((1,), (1,)), ((), ())), preferred_el...  13.4 us
    ppermute x3, starting transfers between devices, from_behind(): return lax.ppermute(shard, axis, pairs)  12.3 us
    dot_general x1, matrix products, on_device(): jnp.dot(normed, lax.all_gather(gate_weight, 'sp', axis=0, tiled=True), pr...  7.64 us
  transfers between devices with their start and end apart: 8, of which 5 were waited for; matrix products, arithmetic and copies ran while one was open for 6% of the time, Pallas kernels for 0%

commit v1 on v0

--- a/solution.py
+++ b/solution.py
@@ -87,7 +87,9 @@
     col_count = model_width // lax.axis_size("tp")
     col_first = lax.axis_index("tp") * col_count
     full_term = jnp.dot(attended, out_weight, preferred_element_type=jnp.float32)
-    projected = lax.psum(full_term.astype(jnp.bfloat16), "tp").astype(jnp.float32)
+    projected = jnp.sum(lax.all_gather(full_term.astype(jnp.bfloat16), "tp"), axis=0).astype(
+        jnp.float32
+    )
     after_full = (residual.astype(jnp.float32) + projected).astype(jnp.bfloat16)
     after_f = after_full.astype(jnp.float32)
     inv_rms = lax.rsqrt(jnp.mean(after_f * after_f, axis=1, keepdims=True) + norm_eps)

time: 368 us -> 425 us (1.15)
  waiting for transfers between devices: 296 us -> 348 us
  other arithmetic: 7.52 us -> 13.9 us
    all_gather x0 -> x1, waiting for transfers between devices: none -> 54.9 us  [on_device(): lax.all_gather(full_term.astype(jnp.bfloat16), 'tp')]
    psum x1 -> x0, waiting for transfers between devices: 48.3 us -> none  [on_device(): lax.psum(full_term.astype(jnp.bfloat16), 'tp').astype(jnp.float32)]
    all_gather x1, waiting for transfers between devices: 40.1 us -> 84.9 us  [on_device(): lax.all_gather(gate_weight, 'sp', axis=0, tiled=True)]
    all_gather x1, waiting for transfers between devices: 92.4 us -> 84.3 us  [on_device(): down_full = lax.all_gather(down_weight, 'sp', axis=0, tiled=True)]
    all_gather x1, waiting for transfers between devices: 84.7 us -> 92.6 us  [on_device(): lax.all_gather(up_weight, 'sp', axis=0, tiled=True)]
    reduce_sum x0 -> x1, other arithmetic: none -> 5.69 us  [on_device(): jnp.sum(lax.all_gather(full_term.astype(jnp.bfloat16), 'tp'), axis=0)]
  transfers between devices with their start and end apart: 8 -> 8, of which waited for: 5 -> 5; matrix products, arithmetic and copies ran while one was open for 6% -> 7% of each run, Pallas kernels for 0% -> 0%
where the time goes in v1:
time: 425 us; the launch traced here: 424 us
  waiting for transfers between devices  348 us (82%)
  matrix products  26.2 us (6%)
  other arithmetic  13.9 us (3%)
  between operations  13.3 us (3%)
  starting transfers between devices  12.7 us (3%)
  local copies, waits for them, and re-layouts  10.2 us (2%)
    all_gather x1, waiting for transfers between devices, on_device(): lax.all_gather(up_weight, 'sp', axis=0, tiled=True)  92.6 us
    all_gather x1, waiting for transfers between devices, on_device(): lax.all_gather(gate_weight, 'sp', axis=0, tiled=True)  84.9 us
    all_gather x1, waiting for transfers between devices, on_device(): down_full = lax.all_gather(down_weight, 'sp', axis=0, tiled=True)  84.3 us
    all_gather x1, waiting for transfers between devices, on_device(): lax.all_gather(full_term.astype(jnp.bfloat16), 'tp')  54.9 us
    reduce_scatter x1, waiting for transfers between devices, on_device(): lax.psum_scatter(lax.dot_general(down_full, hidden, (((1,), (1,)), ((), (...  29.5 us
    dot_general x1, matrix products, on_device(): lax.dot_general(down_full, hidden, (((1,), (1,)), ((), ())), preferred_el...  13.3 us
    ppermute x3, starting transfers between devices, from_behind(): return lax.ppermute(shard, axis, pairs)  12.3 us
  transfers between devices with their start and end apart: 8, of which 5 were waited for; matrix products, arithmetic and copies ran while one was open for 7% of the time, Pallas kernels for 0%

profile of v1, /device:TPU:0, one launch (start us, length us, event | category | flops | bytes accessed | tf_op | source)
XLA Modules:
  0.0 424.3 jit_solution(4557559933703209441)
XLA Ops:
  6.6 0.8 fusion.34
  7.4 4.9 %collective-permute-start.1 = (bf16[128]{0:T(256)(128)(2,1)S(1)}, bf16[128]{0:T(256)(128)(2,1)S(1)}, u32[]{:S(2)}, u32[]{:S(2)}) collective-permute-start(bf16[128]{0:T(256)(128)(2,1)S(1)} %slice.39), channel_id=1, source_target_pairs={{0,4},{4,8},{8,12},{12,16},{16,20},{20,24},{24,28},{1,5},{5,9},{9,... | collective-permute-start | bytes 776 | tf_op jit(solution)/shard_map/ppermute | solution.py:16
  12.3 0.8 slice.42
  13.0 3.4 collective-permute-start.2
  16.5 1.4 slice.36
  17.8 4.0 collective-permute-start
  22.0 1.0 reshape.149
  23.0 1.0 reshape.147
  24.2 2.0 reshape.150
  26.3 0.8 copy.23
  27.4 0.8 copy.18
  28.4 0.6 fusion.17
  29.0 0.7 copy.21
  29.7 1.6 fusion.5
  31.5 0.5 fusion.6
  32.1 0.9 copy.16
  33.0 0.7 fusion.7
  33.9 2.1 convolution_convert_fusion
  36.0 0.7 all-gather.6.cloned.1.call-update
  36.8 0.7 all-gather.10.cloned.1.call-update
  37.5 0.5 all-gather.8.cloned.1.call-update
  38.0 0.2 reduce-scatter.2.cloned.1.call-start
  38.3 54.9 %all-gather.12.cloned.1.call-done = bf16[2048,2048]{1,0:T(8,128)(2,1)} async-done(((bf16[512,2048]{1,0:T(8,128)(2,1)}), bf16[2048,2048]{1,0:T(8,128)(2,1)}) %all-gather.12.cloned.1.call-update) | async-done | bytes 8388624 | tf_op jit(solution)/shard_map/all_gather | solution.py:90
  93.1 5.7 %reduce_sum.31 = bf16[512,2048]{1,0:T(8,128)(2,1)S(1)} reduce(bf16[4,512,2048]{2,1,0:T(8,128)(2,1)} %bitcast.52, bf16[]{:T(256)} %constant.15.clone.1), dimensions={0}, to_apply=%region_2.3 | reduce | flops 3145728 | bytes 10485762 | tf_op jit(solution)/shard_map/reduce_sum | solution.py:90
  98.8 3.9 fusion
  102.8 84.9 %all-gather.6.cloned.1.call-done = bf16[2048,1408]{1,0:T(8,128)(2,1)} async-done(((bf16[256,1408]{1,0:T(8,128)(2,1)}), bf16[2048,1408]{1,0:T(8,128)(2,1)}) %all-gather.6.cloned.1.call-update) | async-done | bytes 5767184 | tf_op jit(solution)/shard_map/all_gather | solution.py:100
  187.6 8.5 %fusion.11 = f32[512,1408]{1,0:T(8,128)} fusion(bf16[2048,1408]{1,0:T(8,128)(2,1)} %all-gather.6.cloned.1.call-done, bf16[512,2048]{1,0:T(8,128)(2,1)} %get-tuple-element.6, f32[2048]{0:T(1024)S(1)} %copy-done.3, f32[512]{0:T(512)S(1)} %add_rsqrt_fusion), kind=kOutput, calls=%fused_computation.22 | convolution fusion | flops 2956984320 | bytes 10758144 | tf_op jit(solution)/shard_map/dot_general | solution.py:98
  196.1 84.3 %all-gather.10.cloned.1.call-done = bf16[2048,1408]{1,0:T(8,128)(2,1)} async-done(((bf16[256,1408]{1,0:T(8,128)(2,1)}), bf16[2048,1408]{1,0:T(8,128)(2,1)}) %all-gather.10.cloned.1.call-update) | async-done | bytes 5767184 | tf_op jit(solution)/shard_map/all_gather | solution.py:108
  280.4 92.6 %all-gather.8.cloned.1.call-done = bf16[2048,1408]{1,0:T(8,128)(2,1)} async-done(((bf16[256,1408]{1,0:T(8,128)(2,1)}), bf16[2048,1408]{1,0:T(8,128)(2,1)}) %all-gather.8.cloned.1.call-update) | async-done | bytes 5767184 | tf_op jit(solution)/shard_map/all_gather | solution.py:105
  372.9 13.3 %fusion.4 = bf16[2048,512]{0,1:T(8,128)(2,1)} fusion(bf16[2048,1408]{1,0:T(8,128)(2,1)} %all-gather.10.cloned.1.call-done, bf16[2048,1408]{1,0:T(8,128)(2,1)} %all-gather.8.cloned.1.call-done, f32[512,1408]{1,0:T(8,128)} %fusion.11, bf16[512,2048]{1,0:T(8,128)(2,1)S(1)} %copy-done.1, f32[2048]{0:T(1024)S(1)} %copy-done.3, f32[512]{0:T(512)S(1)} %add_rsqrt_fusion), kind=kOutput, calls=%fused_computation.10 | convolution fusion | flops 5915148288 | bytes 18622464 | tf_op jit(solution)/shard_map/dot_general | solution.py:111
  386.3 29.5 %reduce-scatter.2.cloned.1.call-done = bf16[512,512]{0,1:T(8,128)(2,1)} async-done(((bf16[2048,512]{0,1:T(8,128)(2,1)}), bf16[512,512]{0,1:T(8,128)(2,1)}) %reduce-scatter.2.cloned.1.call-update) | async-done | bytes 524304 | tf_op jit(solution)/shard_map/reduce_scatter | solution.py:110
  415.8 2.0 fusion.8
  (40 shorter events, 1.4 us)
Async XLA Ops:
  6.5 27.4 %copy-start = (bf16[256,2048]{1,0:T(8,128)(2,1)S(1)}, bf16[256,2048]{1,0:T(8,128)(2,1)}, u32[]{:S(2)}) copy-start(bf16[256,2048]{1,0:T(8,128)(2,1)} %param.17) | copy-start | bytes 3145732
  6.5 19.7 %slice-start = ((bf16[512,128]{1,0:T(8,128)(2,1)}), bf16[384,128]{1,0:T(8,128)(2,1)S(1)}, s32[]{:S(2)}) async-start(bf16[512,128]{1,0:T(8,128)(2,1)} %param.13), calls=%async_computation.6 | async-start | bytes 196608 | tf_op jit(solution)/shard_map/slice | solution.py:27
  6.5 20.8 %slice-start.1 = ((bf16[512,128]{1,0:T(8,128)(2,1)}), bf16[384,128]{1,0:T(8,128)(2,1)S(1)}, s32[]{:S(2)}) async-start(bf16[512,128]{1,0:T(8,128)(2,1)} %param.14), calls=%async_computation.7 | async-start | bytes 196608 | tf_op jit(solution)/shard_map/slice | solution.py:30
  6.5 20.7 %copy-start.4 = (f32[4]{0:T(128)S(1)}, f32[4]{0:T(128)}, u32[]{:S(2)}) copy-start(f32[4]{0:T(128)} %param.16) | copy-start | bytes 52
  6.5 86.6 %all-gather.12.cloned.1.call-start = ((), (), s32[]{:S(2)}) async-start(), calls=%async_computation.5 | async-start | bytes 10485760 | tf_op jit(solution)/shard_map/all_gather | solution.py:90
  7.4 21.0 %collective-permute-start.1 = (bf16[128]{0:T(256)(128)(2,1)S(1)}, bf16[128]{0:T(256)(128)(2,1)S(1)}, u32[]{:S(2)}, u32[]{:S(2)}) collective-permute-start(bf16[128]{0:T(256)(128)(2,1)S(1)} %slice.39), channel_id=1, source_target_pairs={{0,4},{4,8},{8,12},{12,16},{16,20},{20,24},{24,28},{1,5},{5,9},{9,... | collective-permute-start | bytes 776 | tf_op jit(solution)/shard_map/ppermute | solution.py:16
  13.0 16.0 %collective-permute-start.2 = (bf16[128,128]{1,0:T(8,128)(2,1)S(1)}, bf16[128,128]{1,0:T(8,128)(2,1)S(1)}, u32[]{:S(2)}, u32[]{:S(2)}) collective-permute-start(bf16[128,128]{1,0:T(8,128)(2,1)S(1)} %slice.42), channel_id=1, source_target_pairs={{0,4},{4,8},{8,12},{12,16},{16,20},{20,24},{24,28},{1,5},{5,9},{9,... | collective-permute-start | bytes 98312 | tf_op jit(solution)/shard_map/ppermute | solution.py:16
  17.8 14.2 %collective-permute-start = (bf16[128,128]{1,0:T(8,128)(2,1)}, bf16[128,128]{1,0:T(8,128)(2,1)}, u32[]{:S(2)}, u32[]{:S(2)}) collective-permute-start(bf16[128,128]{1,0:T(8,128)(2,1)} %slice.36), channel_id=1, source_target_pairs={{0,4},{4,8},{8,12},{12,16},{16,20},{20,24},{24,28},{1,5},{5,9},{9,... | collective-permute-start | bytes 98312 | tf_op jit(solution)/shard_map/ppermute | solution.py:16
  31.4 1.6 copy-start.2
  36.0 151.7 %all-gather.6.cloned.1.call-start = ((), (), s32[]{:S(2)}) async-start(), calls=%async_computation.1 | async-start | bytes 6488064 | tf_op jit(solution)/shard_map/all_gather | solution.py:100
  36.7 243.6 %all-gather.10.cloned.1.call-start = ((), (), s32[]{:S(2)}) async-start(), calls=%async_computation.3 | async-start | bytes 6488064 | tf_op jit(solution)/shard_map/all_gather | solution.py:108
  37.5 335.4 %all-gather.8.cloned.1.call-start = ((), (), s32[]{:S(2)}) async-start(), calls=%async_computation.2 | async-start | bytes 6488064 | tf_op jit(solution)/shard_map/all_gather | solution.py:105
  38.0 377.7 %reduce-scatter.2.cloned.1.call-start = ((), (), s32[]{:S(2)}) async-start(), calls=%async_computation.4 | async-start | bytes 2621440 | tf_op jit(solution)/shard_map/reduce_scatter | solution.py:110
  98.8 88.8 %copy-start.3 = (f32[2048]{0:T(1024)S(1)}, f32[2048]{0:T(1024)}, u32[]{:S(2)}) copy-start(f32[2048]{0:T(1024)} %param.18) | copy-start | bytes 24580
  187.6 185.3 %copy-start.1 = (bf16[512,2048]{1,0:T(8,128)(2,1)S(1)}, bf16[512,2048]{1,0:T(8,128)(2,1)}, u32[]{:S(2)}) copy-start(bf16[512,2048]{1,0:T(8,128)(2,1)} %get-tuple-element.6) | copy-start | bytes 6291460
Sparse Core Ops, SparseCore 0:
  36.1 56.9 all-gather.11
  95.3 92.2 all-gather.5
  189.8 90.4 all-gather.9
  282.4 90.4 all-gather.7
  386.4 29.3 reduce-scatter.1
